TPU v7x, 512 devices: a whole 4x8x8 slice. The times are simulated.
512 devices in a mesh: fs: 64 (over z, y), tp: 8 (over x, core).
Axes of the slice: x: 4, y: 8, z: 8, core: 2. Of those that a mesh axis runs over, the one named last changes fastest.
Arguments:
- gate_pre: bfloat16 [32768, 3072], P('fs', 'tp'), may hold values from -6 to 6
- up_pre: bfloat16 [32768, 3072], P('fs', 'tp'), may hold values from -6 to 6
- cotangent: bfloat16 [32768, 2048], P('fs'), may hold values from -8 to 8
- gate_weight: bfloat16 [2048, 3072], P('fs', 'tp'), may hold values from -0.125 to 0.125
- up_weight: bfloat16 [2048, 3072], P('fs', 'tp'), may hold values from -0.125 to 0.125
- down_weight: bfloat16 [2048, 3072], P('fs', 'tp'), may hold values from -0.109375 to 0.109375
Outputs:
- grad_input: bfloat16 [32768, 2048], P('fs')
- grad_down: float32 [2048, 3072], P('fs', 'tp')
All inputs are finite; a program needn't handle non-finite values.
Results may differ from a plain program's by a relative error of at most 0.014.
Values may be sent and summed in bfloat16 or wider, within the bound.
A program may use at most 64 MiB of HBM per device.

v0:
```python
import jax
import jax.numpy as jnp
from jax import lax
from jax.sharding import PartitionSpec as P


def sent_together(arrays, axis, dim, along):
    ends, at = ([], 0)
    for a in arrays[:-1]:
        at += a.shape[along]
        ends.append(at)
    both = jnp.concatenate(arrays, axis=along)
    return tuple(jnp.split(lax.all_gather(both, axis, axis=dim, tiled=True), ends, axis=along))


def in_blocks(array, dim, devices):
    dims = array.shape
    parts = array.reshape(*dims[:dim], devices, dims[dim] // devices, *dims[dim + 1 :])
    return jnp.moveaxis(parts, dim, 0)


def sum_at_owner(array, axis, dim):
    parts = in_blocks(array, dim, lax.axis_size(axis))
    arrived = lax.all_to_all(parts, axis, split_axis=0, concat_axis=0, tiled=True)
    return arrived.astype(jnp.float32).sum(axis=0)


def local(gate_pre, up_pre, cotangent, gate_weight, up_weight, down_weight):
    gate = gate_pre.astype(jnp.float32)
    upper = up_pre.astype(jnp.float32)
    sigma = jax.nn.sigmoid(gate)
    hidden = (gate * sigma * upper).astype(jnp.bfloat16)
    down_full, gate_full, up_full = sent_together((down_weight, gate_weight, up_weight), "fs", 0, 1)
    d_hidden = jnp.dot(cotangent, down_full, preferred_element_type=jnp.float32)
    d_gate = (d_hidden * upper * sigma * (1.0 + gate * (1.0 - sigma))).astype(jnp.bfloat16)
    d_up = (d_hidden * gate * sigma).astype(jnp.bfloat16)
    first = lax.dot_general(
        d_gate, gate_full, (((1,), (1,)), ((), ())), preferred_element_type=jnp.float32
    )
    partial_sum = first + lax.dot_general(
        d_up, up_full, (((1,), (1,)), ((), ())), preferred_element_type=jnp.float32
    )
    block_part = partial_sum.astype(jnp.bfloat16)
    grad_input = lax.psum(block_part, "tp").astype(jnp.float32).astype(jnp.bfloat16)
    grad_down = sum_at_owner(
        lax.dot_general(
            cotangent, hidden, (((0,), (0,)), ((), ())), preferred_element_type=jnp.float32
        ).astype(jnp.bfloat16),
        "fs",
        0,
    )
    return (grad_input, grad_down)


def solution(mesh):
    placed = (
        P("fs", "tp"),
        P("fs", "tp"),
        P("fs", None),
        P("fs", "tp"),
        P("fs", "tp"),
        P("fs", "tp"),
    )
    return jax.shard_map(
        local, mesh=mesh, in_specs=placed, out_specs=(P("fs", None), P("fs", "tp")), check_vma=False
    )
```

profile of v0, /device:TPU:1, one launch (start us, length us, event | category | flops | bytes accessed | tf_op | source)
XLA Modules:
  0.0 218.4 jit_solution(5023479573007827027)
XLA Ops:
  7.2 0.0 copy-start
  7.2 0.0 all-gather.2.cloned.1.call-start
  7.2 1.5 pad_maximum_fusion
  8.8 0.0 all-gather.2.cloned.1.call-update
  8.8 1.2 copy.11
  10.0 1.2 copy.10
  11.1 0.0 copy-done
  11.1 2.2 %fusion = bf16[2048,384]{0,1:T(8,128)(2,1)} fusion(bf16[512,2048]{1,0:T(8,128)(2,1)S(1)} %copy-done, bf16[512,384]{0,1:T(8,128)(2,1)S(1)} %copy.10, bf16[512,384]{0,1:T(8,128)(2,1)S(1)} %copy.11), kind=kOutput, calls=%fused_computation.3 | convolution fusion | flops 807665664 | bytes 4456448 | tf_op jit(solution)/shard_map/dot_general | solution.py:46
  13.3 2.6 %copy.12 = bf16[2048,384]{1,0:T(8,128)(2,1)} copy(bf16[2048,384]{0,1:T(8,128)(2,1)} %fusion) | data formatting | bytes 3145728 | tf_op jit(solution)/shard_map/convert_element_type | solution.py:48
  15.9 17.4 %all-to-all-start = ((bf16[64,32,384]{2,1,0:T(8,128)(2,1)}), bf16[64,32,384]{2,1,0:T(8,128)(2,1)}, u32[]{:S(2)}, u32[]{:S(2)}) async-start(bf16[64,32,384]{2,1,0:T(8,128)(2,1)} %bitcast.7), calls=%async_computation | async-start | bytes 3145728 | tf_op jit(solution)/shard_map/all_to_all | solution.py:24
  33.3 0.0 all-reduce.2.cloned.1.call-start
  33.3 92.6 %all-gather.2.cloned.1.call-done = bf16[2048,1152]{1,0:T(8,128)(2,1)} async-done(((bf16[32,1152]{1,0:T(8,128)(2,1)}), bf16[2048,1152]{1,0:T(8,128)(2,1)}) %all-gather.2.cloned.1.call-update) | async-done | bytes 4718608 | tf_op jit(solution)/shard_map/all_gather | solution.py:13
  125.9 0.0 copy-start.1
  125.9 2.6 %fusion.6 = f32[512,384]{0,1:T(8,128)S(1)} fusion(bf16[512,2048]{1,0:T(8,128)(2,1)S(1)} %copy-done, bf16[2048,1152]{1,0:T(8,128)(2,1)} %all-gather.2.cloned.1.call-done), kind=kOutput, calls=%fused_computation.13 | convolution fusion | flops 805306368 | bytes 4456448 | tf_op jit(solution)/shard_map/dot_general | solution.py:34
  128.5 0.2 copy-done.1
  128.8 1.5 fusion.2
  130.2 2.6 %add_convert_fusion = bf16[512,2048]{1,0:T(8,128)(2,1)} fusion(f32[512,2048]{1,0:T(8,128)S(1)} %fusion.2, bf16[2048,1152]{1,0:T(8,128)(2,1)S(1)} %copy-done.1, f32[512,384]{0,1:T(8,128)S(1)} %fusion.6, bf16[512,384]{0,1:T(8,128)(2,1)S(1)} %copy.11), kind=kOutput, calls=%fused_computation | convolution fusion | flops 808779776 | bytes 9043968 | tf_op jit(solution)/shard_map/dot_general | solution.py:40
  132.9 0.0 all-reduce.2.cloned.1.call-update
  132.9 0.0 all-to-all-done
  132.9 2.3 %convert_reduce_fusion = f32[32,384]{1,0:T(8,128)} fusion(bf16[64,32,384]{2,1,0:T(8,128)(2,1)} %all-to-all-done), kind=kLoop, calls=%fused_computation.1 | loop fusion | flops 1560576 | bytes 1622016 | tf_op jit(solution)/shard_map/reduce_sum | solution.py:25
  135.2 73.2 %all-reduce.2.cloned.1.call-done = bf16[512,2048]{1,0:T(8,128)(2,1)} async-done(((bf16[512,2048]{1,0:T(8,128)(2,1)}), bf16[512,2048]{1,0:T(8,128)(2,1)}) %all-reduce.2.cloned.1.call-update) | async-done | bytes 2097168 | tf_op jit(solution)/shard_map/psum | solution.py:44
  208.4 3.2 %copy.14 = bf16[512,2048]{1,0:T(8,128)(2,1)} copy(bf16[512,2048]{1,0:T(8,128)(2,1)} %all-reduce.2.cloned.1.call-done) | data formatting | bytes 4194304
Async XLA Ops:
  7.2 4.0 %copy-start = (bf16[512,2048]{1,0:T(8,128)(2,1)S(1)}, bf16[512,2048]{1,0:T(8,128)(2,1)}, u32[]{:S(2)}) copy-start(bf16[512,2048]{1,0:T(8,128)(2,1)} %param.8) | copy-start | bytes 6291460
  7.2 118.8 %all-gather.2.cloned.1.call-start = ((), (), s32[]{:S(2)}) async-start(), calls=%async_computation.1 | async-start | bytes 4792320 | tf_op jit(solution)/shard_map/all_gather | solution.py:13
  15.9 117.0 %all-to-all-start = ((bf16[64,32,384]{2,1,0:T(8,128)(2,1)}), bf16[64,32,384]{2,1,0:T(8,128)(2,1)}, u32[]{:S(2)}, u32[]{:S(2)}) async-start(bf16[64,32,384]{2,1,0:T(8,128)(2,1)} %bitcast.7), calls=%async_computation | async-start | bytes 3145728 | tf_op jit(solution)/shard_map/all_to_all | solution.py:24
  33.3 175.1 %all-reduce.2.cloned.1.call-start = ((), (), s32[]{:S(2)}) async-start(), calls=%async_computation.2 | async-start | bytes 4194304 | tf_op jit(solution)/shard_map/psum | solution.py:44
  125.9 2.8 %copy-start.1 = (bf16[2048,1152]{1,0:T(8,128)(2,1)S(1)}, bf16[2048,1152]{1,0:T(8,128)(2,1)}, u32[]{:S(2)}) copy-start(bf16[2048,1152]{1,0:T(8,128)(2,1)} %all-gather.2.cloned.1.call-done) | copy-start | bytes 14155780
Sparse Core Ops, SparseCore 0:
  11.0 114.9 all-gather.1
  133.0 75.3 all-reduce.1
where the time goes:
time: 220 us; the launch traced here: 218 us
  waiting for transfers between devices  166 us (75%)
  starting transfers between devices  17.4 us (8%)
  between operations  14.1 us (6%)
  matrix products  8.88 us (4%)
  local copies, waits for them, and re-layouts  8.31 us (4%)
  other arithmetic  3.81 us (2%)
    all_gather x1, waiting for transfers between devices, sent_together(): lax.all_gather(both, axis, axis=dim, tiled=True)  92.6 us
    psum x1, waiting for transfers between devices, local(): lax.psum(block_part, 'tp').astype(jnp.float32).astype(jnp.bfloat16)  73.2 us
    all_to_all x1, starting transfers between devices, sum_at_owner(): lax.all_to_all(parts, axis, split_axis=0, concat_axis=0, tiled=True)  17.4 us
    unnamed x7, local copies, waits for them, and re-layouts  5.74 us
  transfers between devices with their start and end apart: 3, of which 2 were waited for; matrix products, arithmetic and copies ran while one was open for 7% of the time, Pallas kernels for 0%

commit v1 on v0

v1 whole, which is shorter than its diff:
```python
import functools

import jax
import jax.numpy as jnp
from jax import lax
from jax.experimental import pallas as pl
from jax.experimental.pallas import tpu as pltpu
from jax.sharding import PartitionSpec as P

MESH = pl.DeviceIdType.MESH
f32, bf16 = jnp.float32, jnp.bfloat16
N = 8
X = 4
T, D, F = 512, 2048, 384
H = 16
A, B = 0, 1
DOWN, GATE, UP = 0, 1, 2
LONG = {DOWN: -1, GATE: 1, UP: -1}
RS_LONG = 1
LAGS = (1, 3, 5, 7, 9, 10)


def reach(m, sign):
    return 4 if LONG[m] == sign else 3


def rs_reach(sign):
    return 4 if RS_LONG == sign else 3


def chunk_order():
    order = [(A, 1, 0), (B, 1, 0)]
    for k in (1, 2, 3):
        order += [(r, s, k) for r in (A, B) for s in (1, -1)]
    return order + [(A, 1, 4), (B, 1, 4)]


def kernel(
    gate_hbm, up_hbm, cot_hbm, wd_hbm, wg_hbm, wu_hbm,
    ot_hbm, gd_ref,
    gate, up, cot, w, hid, fa, fb, dg, du, g, rs_out, rs_in, lt_tot, lt_out, lt_in,
    part, dr, xs, xr, ot,
    load_sem, out_sem, ssem, rsem,
):
    fs, tp = lax.axis_index("fs"), lax.axis_index("tp")
    z, y = fs // N, fs % N
    x, c = tp // 2, tp % 2
    keys, sends = {}, []

    def ring(i):
        return lax.rem(i + N, N)

    def xring(i):
        return lax.rem(i + X, X)

    def at(zz, yy):
        return {"fs": zz * N + yy, "tp": tp}

    def along(xx, cc):
        return {"fs": fs, "tp": xx * 2 + cc}

    partner = along(x, 1 - c)

    def sem_of(key):
        return keys.setdefault(key, len(keys))

    def send(src, dst, device, key):
        i = sem_of(key)
        d = pltpu.make_async_remote_copy(src, dst, ssem.at[i], rsem.at[i], device_id=device, device_id_type=MESH)
        d.start()
        sends.append(d)

    def recv(dst, key):
        i = sem_of(key)
        pltpu.make_async_remote_copy(dst, dst, ssem.at[i], rsem.at[i], device_id=partner, device_id_type=MESH).wait_recv()

    loads = [pltpu.make_async_copy(src, w.at[m, z, y], load_sem.at[m]) for m, src in enumerate((wd_hbm, wg_hbm, wu_hbm))]
    loads += [pltpu.make_async_copy(gate_hbm, gate, load_sem.at[3]), pltpu.make_async_copy(up_hbm, up, load_sem.at[4])]
    loads += [pltpu.make_async_copy(cot_hbm, cot, load_sem.at[5])]
    for copy in loads:
        copy.start()
    barrier = pltpu.get_barrier_semaphore()
    peers = [at(z, ring(y + o)) for o in range(1, N)] + [at(ring(z + o), y) for o in range(1, N)]
    peers += [along(xring(x + 1), c), along(xring(x - 1), c), partner]
    for peer in peers:
        pl.semaphore_signal(barrier, inc=1, device_id=peer, device_id_type=MESH)
    for m in range(3):
        loads[m].wait()
    pl.semaphore_wait(barrier, len(peers))

    def first_ref(m, r, o):
        return w.at[m, z, ring(y + o), pl.ds(0, H)] if r == A else w.at[m, ring(z + o), y, pl.ds(H, H)]

    def first_send(m):
        for o in (4, 3, 5, 2, 6, 1, 7):
            for r in (A, B):
                ref = first_ref(m, r, 0)
                send(ref, ref, at(z, ring(y + o)) if r == A else at(ring(z + o), y), ("p1", m, r, o))

    def first_wait(m):
        for o in (1, 7, 2, 6, 3, 5, 4):
            for r in (A, B):
                recv(first_ref(m, r, -o), ("p1", m, r, o))

    def group(m, r, i):
        return w.at[m, ring(z + i), :, pl.ds(0, H)] if r == A else w.at[m, :, ring(y + i), pl.ds(H, H)]

    def second_send(m, r, s, k):
        if k > reach(m, s):
            return
        ref = group(m, r, -s * (k - 1))
        send(ref, ref, at(ring(z + s), y) if r == A else at(z, ring(y + s)), ("p2", m, r, s, k))

    def second_recv(m, r, s, k):
        if k <= reach(m, s):
            recv(group(m, r, -s * k), ("p2", m, r, s, k))

    ALL = [(r, s) for r in (A, B) for s in (1, -1)]

    for m in (DOWN, GATE, UP):
        first_send(m)

    loads[3].wait()
    loads[4].wait()

    @pl.loop(0, T // 64)
    def _(i):
        rows = pl.ds(pl.multiple_of(i * 64, 64), 64)
        gv, uv = gate[rows].astype(f32), up[rows].astype(f32)
        sv = jax.nn.sigmoid(gv)
        gs = gv * sv
        hid[rows] = (gs * uv).astype(bf16)
        fa[rows] = uv * sv * (1.0 + gv * (1.0 - sv))
        fb[rows] = gs

    loads[5].wait()

    @pl.loop(0, N)
    def _(i):
        columns = pl.ds(pl.multiple_of(i * 256, 256), 256)
        block = lax.dot_general(cot[:, columns], hid[...], (((0,), (0,)), ((), ())), preferred_element_type=f32)
        g[i] = block.reshape(N, 2 * H, F)

    def own(r, i):
        return g[:, ring(y + i), pl.ds(0, H)] if r == A else g[ring(z + i), :, pl.ds(H, H)]

    def slot(s, k):
        return (0 if s == 1 else 4) + k - 1

    def rs_send(r, s, k):
        if k > rs_reach(s):
            return
        value = own(r, s * (rs_reach(s) - k + 1))
        if k > 1:
            value = value + rs_in[r, slot(s, k - 1)].astype(f32)
        rs_out[r, slot(s, k)] = value.astype(bf16)
        device = at(z, ring(y + s)) if r == A else at(ring(z + s), y)
        send(rs_out.at[r, slot(s, k)], rs_in.at[r, slot(s, k)], device, ("rs", r, s, k))

    def rs_recv(r, s, k):
        if k <= rs_reach(s):
            recv(rs_in.at[r, slot(s, k)], ("rs", r, s, k))

    def light_send(r):
        total = own(r, 0) + rs_in[r, slot(1, rs_reach(1))].astype(f32) + rs_in[r, slot(-1, rs_reach(-1))].astype(f32)
        lt_tot[r] = total
        lt_out[r] = total.astype(bf16)
        me = z if r == A else y
        for o in (4, 3, 5, 2, 6, 1, 7):
            device = at(ring(z + o), y) if r == A else at(z, ring(y + o))
            send(lt_out.at[r, ring(me + o)], lt_in.at[r, me], device, ("lt", r, o))

    def light_finish(r):
        me = z if r == A else y
        total = lt_tot[r, me]
        for o in range(1, N):
            recv(lt_in.at[r, ring(me - o)], ("lt", r, o))
            total = total + lt_in[r, ring(me - o)].astype(f32)
        gd_ref[pl.ds(r * H, H)] = total

    first_wait(DOWN)
    for r, s in ALL:
        second_send(DOWN, r, s, 1)
    for r, s in ALL:
        rs_send(r, s, 1)
    first_wait(GATE)
    first_wait(UP)
    for k in (1, 2, 3, 4):
        for r, s in ALL:
            second_recv(DOWN, r, s, k)
            second_send(DOWN, r, s, k + 1)
        for r, s in ALL:
            rs_recv(r, s, k)
            rs_send(r, s, k + 1)
        if k == 2:
            for r, s in ALL:
                second_send(GATE, r, s, 1)
        if k == 3:
            for r, s in ALL:
                second_send(UP, r, s, 1)

    d_hidden = jnp.dot(cot[...], w[DOWN].reshape(D, F), preferred_element_type=f32)
    dg[...] = (d_hidden * fa[...]).astype(bf16)
    du[...] = (d_hidden * fb[...]).astype(bf16)
    for r in (A, B):
        light_send(r)

    order = chunk_order()
    outs = []

    def way(i):
        return 1 if i % 2 == 0 else -1

    def piece(i, q, n=None):
        r, s, k = order[i]
        q = q if n is None else pl.ds(q, n)
        if r == A:
            return ot.at[ring(z - s * k), q, pl.ds(0, H)]
        return ot.at[q, ring(y - s * k), pl.ds(H, H)]

    def arrive(i):
        r, s, k = order[i]
        if k == 0:
            return
        for m in (GATE, UP):
            for ss in (1, -1) if k == 4 else (s,):
                second_recv(m, r, ss, k)
                second_send(m, r, ss, k + 1)

    def sums(i, j):
        return part[i, c * X + j].astype(f32) + dr[i, j].astype(f32)

    def stage0(i):
        r, s, k = order[i]
        arrive(i)

        def rows_of(m):
            v = w[m, ring(z - s * k), :, pl.ds(0, H)] if r == A else w[m, :, ring(y - s * k), pl.ds(H, H)]
            return v.reshape(N * H, F)

        nt = (((1,), (1,)), ((), ()))
        p = lax.dot_general(rows_of(GATE), dg[...], nt, preferred_element_type=f32)
        p = p + lax.dot_general(rows_of(UP), du[...], nt, preferred_element_type=f32)
        part[i] = p.astype(bf16).reshape(N, H, T)
        send(part.at[i, pl.ds((1 - c) * X, X)], dr.at[i], partner, ("d2d", i))

    def stage1(i):
        s = way(i)
        recv(dr.at[i], ("d2d", i))
        xs[i, 0] = sums(i, xring(x + 2)).astype(bf16)
        send(xs.at[i, 0], xr.at[i, 0], along(xring(x + s), c), ("x1", i))
        xs[i, 1] = sums(i, xring(x - s)).astype(bf16)
        send(xs.at[i, 1], xr.at[i, 1], along(xring(x - s), c), ("x2", i))

    def stage2(i):
        s = way(i)
        recv(xr.at[i, 0], ("x1", i))
        xs[i, 2] = (sums(i, xring(x + s)) + xr[i, 0].astype(f32)).astype(bf16)
        send(xs.at[i, 2], xr.at[i, 2], along(xring(x + s), c), ("x3", i))

    def stage3(i):
        recv(xr.at[i, 1], ("x2", i))
        recv(xr.at[i, 2], ("x3", i))
        total = sums(i, x) + xr[i, 1].astype(f32) + xr[i, 2].astype(f32)
        mine = piece(i, c * X + x)
        mine[...] = total.astype(bf16)
        for s in (1, -1):
            send(mine, mine, along(xring(x + s), c), ("g1", i, s))

    def stage4(i):
        s = way(i)
        behind = piece(i, c * X + xring(x - s))
        recv(behind, ("g1", i, s))
        send(behind, behind, along(xring(x + s), c), ("g2", i))
        recv(piece(i, c * X + xring(x + s)), ("g1", i, -s))

    def stage5(i):
        recv(piece(i, c * X + xring(x + 2)), ("g2", i))
        half = piece(i, c * X, X)
        send(half, half, partner, ("g3", i))

    def stage6(i):
        recv(piece(i, (1 - c) * X, X), ("g3", i))
        r, s, k = order[i]
        if r == A:
            src, dst = (ref.at[ring(z - s * k), :, pl.ds(0, H)] for ref in (ot, ot_hbm))
        else:
            src, dst = (ref.at[:, ring(y - s * k), pl.ds(H, H)] for ref in (ot, ot_hbm))
        copy = pltpu.make_async_copy(src, dst, out_sem.at[i])
        copy.start()
        outs.append(copy)

    stages = (stage1, stage2, stage3, stage4, stage5, stage6)
    chunks = len(order)
    for i in range(chunks + LAGS[-1]):
        for lag, stage in reversed(list(zip(LAGS, stages))):
            if 0 <= i - lag < chunks:
                stage(i - lag)
        if i < chunks:
            stage0(i)
        if i == 8:
            for r in (A, B):
                light_finish(r)

    for d in sends:
        d.wait_send()
    for copy in outs:
        copy.wait()


SEMS = 240


def local(gate_pre, up_pre, cotangent, gate_weight, up_weight, down_weight):
    hbm = pl.BlockSpec(memory_space=pltpu.HBM)
    ot, grad_down = pl.pallas_call(
        kernel,
        out_shape=(jax.ShapeDtypeStruct((N, N, 2 * H, T), bf16), jax.ShapeDtypeStruct((2 * H, F), f32)),
        in_specs=[hbm] * 6,
        out_specs=(hbm, pl.BlockSpec(memory_space=pltpu.VMEM)),
        scratch_shapes=[
            pltpu.VMEM((T, F), bf16),
            pltpu.VMEM((T, F), bf16),
            pltpu.VMEM((T, D), bf16),
            pltpu.VMEM((3, N, N, 2 * H, F), bf16),
            pltpu.VMEM((T, F), bf16),
            pltpu.VMEM((T, F), f32),
            pltpu.VMEM((T, F), f32),
            pltpu.VMEM((T, F), bf16),
            pltpu.VMEM((T, F), bf16),
            pltpu.VMEM((N, N, 2 * H, F), f32),
            pltpu.VMEM((2, 7, N, H, F), bf16),
            pltpu.VMEM((2, 7, N, H, F), bf16),
            pltpu.VMEM((2, N, H, F), f32),
            pltpu.VMEM((2, N, H, F), bf16),
            pltpu.VMEM((2, N, H, F), bf16),
            pltpu.VMEM((16, N, H, T), bf16),
            pltpu.VMEM((16, X, H, T), bf16),
            pltpu.VMEM((16, 3, H, T), bf16),
            pltpu.VMEM((16, 3, H, T), bf16),
            pltpu.VMEM((N, N, 2 * H, T), bf16),
            pltpu.SemaphoreType.DMA((6,)),
            pltpu.SemaphoreType.DMA((16,)),
            pltpu.SemaphoreType.DMA((SEMS,)),
            pltpu.SemaphoreType.DMA((SEMS,)),
        ],
        compiler_params=pltpu.CompilerParams(
            collective_id=0, has_side_effects=True, vmem_limit_bytes=60 * 1024 * 1024
        ),
    )(gate_pre, up_pre, cotangent, down_weight, gate_weight, up_weight)
    return ot.reshape(D, T).T, grad_down


def solution(mesh):
    placed = (P("fs", "tp"), P("fs", "tp"), P("fs", None), P("fs", "tp"), P("fs", "tp"), P("fs", "tp"))
    return jax.shard_map(
        local, mesh=mesh, in_specs=placed, out_specs=(P("fs", None), P("fs", "tp")), check_vma=False
    )
```

time: 220 us -> 93.9 us (0.43)
  waiting for transfers between devices: 166 us -> 0 us
  Pallas kernels: 0 us -> 88.5 us
  starting transfers between devices: 17.4 us -> 0 us
  between operations: 14.1 us -> 0.65 us
  matrix products: 8.88 us -> 0 us
  other arithmetic: 3.81 us -> 0 us
  local copies, waits for them, and re-layouts: 8.31 us -> 4.54 us
    all_gather x1 -> x0, waiting for transfers between devices: 92.6 us -> none  [sent_together(): lax.all_gather(both, axis, axis=dim, tiled=True)]
    pallas_call x0 -> x1, Pallas kernels: none -> 88.5 us  [local(): pl.pallas_call(kernel, out_shape=(jax.ShapeDtypeStruct((N, N, 2 * H, T),...]
    psum x1 -> x0, waiting for transfers between devices: 73.2 us -> none  [local(): lax.psum(block_part, 'tp').astype(jnp.float32).astype(jnp.bfloat16)]
    all_to_all x1 -> x0, starting transfers between devices: 17.4 us -> none  [sum_at_owner(): lax.all_to_all(parts, axis, split_axis=0, concat_axis=0, tiled=True)]
    dot_general x4 -> x0, matrix products: 8.88 us -> none  [the longest x1 2.65 us: local(): lax.dot_general(d_up, up_full, (((1,), (1,)), ((), ())), preferred_elemen...]
    unnamed x7 -> x3, local copies, waits for them, and re-layouts: 5.74 us -> 0.62 us
    reshape x0 -> x1, local copies, waits for them, and re-layouts: none -> 3.92 us  [local(): return (ot.reshape(D, T).T, grad_down)]
    convert_element_type x1 -> x0, local copies, waits for them, and re-layouts: 2.57 us -> none  [local(): grad_down = sum_at_owner(lax.dot_general(cotangent, hidden, (((0,), (0,))...]
  transfers between devices with their start and end apart: 3 -> 0, of which waited for: 2 -> 0; matrix products, arithmetic and copies ran while one was open for 7% -> 0% of each run, Pallas kernels for 0% -> 0%
where the time goes in v1:
time: 93.9 us; the launch traced here: 93.7 us
  Pallas kernels  88.5 us (94%)
  local copies, waits for them, and re-layouts  4.54 us (5%)
    pallas_call x1, Pallas kernels, local(): pl.pallas_call(kernel, out_shape=(jax.ShapeDtypeStruct((N, N, 2 * H, T),...  88.5 us
    reshape x1, local copies, waits for them, and re-layouts, local(): return (ot.reshape(D, T).T, grad_down)  3.92 us

profile of v1, /device:TPU:1, one launch (start us, length us, event | category | flops | bytes accessed | tf_op | source)
XLA Modules:
  0.0 93.7 jit_solution(13786650063854764814)
XLA Ops:
  0.6 88.5 %shard_map.77 = (bf16[8,8,32,512]{3,2,1,0:T(8,128)(2,1)}, f32[32,384]{1,0:T(8,128)}) custom-call(bf16[512,384]{1,0:T(8,128)(2,1)} %gate_hbm.1, bf16[512,384]{1,0:T(8,128)(2,1)} %up_hbm.1, bf16[512,2048]{1,0:T(8,128)(2,1)} %cot_hbm.1, bf16[32,384]{1,0:T(8,128)(2,1)} %wd_hbm.1, bf16[32,384]{1,0:T(8,128)(2,1)} %wg_hbm.1, bf16[32,384]{1,0:T(8,128)(2,1)} %wu_hbm.1), custom_call_target="tpu_custom_call" | custom-call | tf_op jit(solution)/shard_map/pallas_call | solution.py:316
  89.2 0.0 copy-start
  89.2 3.9 %copy.8 = bf16[2048,512]{0,1:T(8,128)(2,1)} copy(bf16[2048,512]{1,0:T(8,128)(2,1)} %bitcast.3) | data formatting | bytes 4194304 | tf_op jit(solution)/shard_map/reshape | solution.py:351
  93.1 0.0 copy-done
  93.1 0.6 copy.10
Async XLA Ops:
  89.2 3.9 %copy-start = (f32[32,384]{1,0:T(8,128)S(1)}, f32[32,384]{1,0:T(8,128)}, u32[]{:S(2)}) copy-start(f32[32,384]{1,0:T(8,128)} %get-tuple-element.9) | copy-start | bytes 147460
